TPU v7x, 32 devices: a whole 2x2x4 slice. The times are simulated.
32 devices in a mesh: ep: 8 (over z, core), tp: 4 (over y, x).
Axes of the slice: x: 2, y: 2, z: 4, core: 2. Of those that a mesh axis runs over, the one named last changes fastest.
Arguments:
- queries: bfloat16 [2048, 4096], P('ep', 'tp'), may hold values from -6 to 6
- keys: bfloat16 [2048, 1024], P('ep', 'tp'), may hold values from -6 to 6
- values: bfloat16 [2048, 1024], P('ep', 'tp'), may hold values from -6 to 6
- query_gain: float32 [64], replicated, may hold values from 1 to 11
- key_gain: float32 [64], replicated, may hold values from 1 to 11
- moe_rows: bfloat16 [2048, 4096], P('ep', 'tp'), may hold values from -14 to 14
- route_ids: int32 [2048, 2], P('ep'), may hold values from 0 to 7, all different within a row; in each aligned block of 256 rows (0 to 255, 256 to 511, ...) at most 96 rows name the same one
- group_weight: float32 [2048], P('ep'), may hold values from 0.2 to 1
- expert_weight: float32 [2048, 2], P('ep'), may hold values from 0.05 to 1
- expert_gate: bfloat16 [8, 4096, 2048], P('ep', None, 'tp'), may hold values from -0.09375 to 0.09375
- expert_up: bfloat16 [8, 4096, 2048], P('ep', None, 'tp'), may hold values from -0.09375 to 0.09375
- expert_down: bfloat16 [8, 2048, 4096], P('ep', None, 'tp'), may hold values from -0.125 to 0.125
Outputs:
- attended: bfloat16 [2048, 4096], P('ep', 'tp')
- moe_out: bfloat16 [2048, 4096], P('ep', 'tp')
Inputs may be any that keep to these rules, and one draw needn't show every extreme that they name: `route_ids`: each row names 2 different experts. Among the rows of one device no expert is named by more than 96 rows, and in every draw some expert is named by exactly 96 of them.
All inputs are finite; a program needn't handle non-finite values.
Results may differ from a plain program's by a relative error of at most 0.0055.
The roundings to bfloat16 on the way count: a program that leaves them out, or rounds other values in their place, can miss the bound.
Values may be sent and summed in bfloat16 or wider, within the bound.
A program may use at most 128 MiB of HBM per device.

v0:
```python
import jax
import jax.numpy as jnp
from jax import lax
from jax.sharding import PartitionSpec as P

D = 4096
HEAD_DIM = 64
GRID_W = 64
TOPK = 2


def rotary_tables(position):
    pair_count = HEAD_DIM // 4
    grid_pos = jnp.stack([position // GRID_W, position % GRID_W], axis=-1).astype(jnp.float32)
    frequency = 10000.0 ** (-jnp.arange(pair_count, dtype=jnp.float32) / pair_count)
    angles = grid_pos[:, :, None] * frequency
    return (jnp.cos(angles), jnp.sin(angles))


def normed_rotated(rows_in, gain, cosine, sine_of):
    row_count, head_count = (rows_in.shape[0], rows_in.shape[1])
    pair_count = HEAD_DIM // 4
    scaled = rows_in * lax.rsqrt(jnp.mean(rows_in * rows_in, axis=-1, keepdims=True) + 1e-06) * gain
    parted = scaled.reshape(row_count, head_count, 2, 2, pair_count)
    first_half, second = (parted[:, :, :, 0, :], parted[:, :, :, 1, :])
    cos_b, sin_b = (cosine[:, None], sine_of[:, None])
    turned = jnp.stack(
        [first_half * cos_b - second * sin_b, second * cos_b + first_half * sin_b], axis=3
    )
    return turned.reshape(row_count, head_count, HEAD_DIM).astype(jnp.bfloat16)


def attend_block(carried, portion, query_rot, kv_width):
    running_max, denominator, summed = carried
    key_count = portion.shape[0]
    head_count = kv_width // HEAD_DIM
    keys_part = portion[:, :kv_width].reshape(key_count, head_count, HEAD_DIM)
    values_part = portion[:, kv_width:].reshape(key_count, head_count, HEAD_DIM)
    scores = jnp.einsum(
        "tkgd,skd->kgts", query_rot, keys_part, preferred_element_type=jnp.float32
    ) * HEAD_DIM ** (-0.5)
    new_max = jnp.max(scores, axis=-1)
    factor = jnp.exp(running_max - new_max)
    weights = jnp.exp(scores - new_max[..., None])
    denominator = denominator * factor + jnp.sum(weights, axis=-1)
    summed = summed * factor[..., None] + jnp.einsum(
        "kgts,skd->kgtd",
        weights.astype(jnp.bfloat16),
        values_part,
        preferred_element_type=jnp.float32,
    )
    return (new_max, denominator, summed)


def on_device(
    queries,
    keys,
    values,
    query_gain,
    key_gain,
    moe_rows,
    route_ids,
    group_weight,
    expert_weight,
    expert_gate,
    expert_up,
    expert_down,
):
    tok_rows = queries.shape[0]
    q_heads = queries.shape[1] // HEAD_DIM
    k_heads = keys.shape[1] // HEAD_DIM
    group_size = q_heads // k_heads
    position = lax.axis_index("ep") * tok_rows + jnp.arange(tok_rows, dtype=jnp.int32)
    cosine, sine_of = rotary_tables(position)
    query_rot = normed_rotated(
        queries.astype(jnp.float32).reshape(tok_rows, q_heads, HEAD_DIM),
        query_gain,
        cosine,
        sine_of,
    )
    query_rot = query_rot.reshape(tok_rows, k_heads, group_size, HEAD_DIM)
    key_rot = normed_rotated(
        keys.astype(jnp.float32).reshape(tok_rows, k_heads, HEAD_DIM), key_gain, cosine, sine_of
    )
    kv_width = k_heads * HEAD_DIM
    joined = jnp.concatenate([key_rot.reshape(tok_rows, kv_width), values], axis=1)
    initial = (
        jnp.full((k_heads, group_size, tok_rows), -jnp.inf, jnp.float32),
        jnp.zeros((k_heads, group_size, tok_rows), jnp.float32),
        jnp.zeros((k_heads, group_size, tok_rows, HEAD_DIM), jnp.float32),
    )
    final_max, denominator, summed = attend_block(
        initial, lax.all_gather(joined, "ep", axis=0, tiled=True), query_rot, kv_width
    )
    attended = (
        (summed / denominator[..., None])
        .transpose(2, 0, 1, 3)
        .reshape(tok_rows, q_heads * HEAD_DIM)
        .astype(jnp.bfloat16)
    )
    moe_tokens = moe_rows.shape[0]
    local_experts = expert_gate.shape[0]
    expert_count = local_experts * lax.axis_size("ep")
    capacity = 3 * moe_tokens * TOPK // (2 * expert_count)
    picks = moe_tokens * TOPK
    route_list = route_ids.reshape(picks)
    one_hot = (route_list[:, None] == jnp.arange(expert_count, dtype=jnp.int32)[None, :]).astype(
        jnp.int32
    )
    rank_of = jnp.sum((jnp.cumsum(one_hot, axis=0) - one_hot) * one_hot, axis=1)
    slot_of = route_list * capacity + rank_of
    owner_of = (
        jnp.full((expert_count * capacity,), moe_tokens, jnp.int32)
        .at[slot_of]
        .set(jnp.arange(picks, dtype=jnp.int32) // TOPK)
    )
    padded = jnp.concatenate([moe_rows, jnp.zeros((1, moe_rows.shape[1]), moe_rows.dtype)], axis=0)
    arrived = lax.all_to_all(
        padded[owner_of].reshape(expert_count, capacity, moe_rows.shape[1]),
        "ep",
        split_axis=0,
        concat_axis=1,
        tiled=True,
    )
    portion = lax.all_gather(arrived, "tp", axis=2, tiled=True)
    widened = portion.astype(jnp.float32)
    gate_act = jnp.einsum("erd,edf->erf", portion, expert_gate, preferred_element_type=jnp.float32)
    up_act = jnp.einsum("erd,edf->erf", portion, expert_up, preferred_element_type=jnp.float32)
    square_sum = jnp.sum(widened * widened, axis=2)
    inv_rms = lax.rsqrt(square_sum / D + 1e-06)[..., None]
    hidden = (jax.nn.silu(gate_act * inv_rms) * (up_act * inv_rms)).astype(jnp.bfloat16)
    out_cols = expert_down.shape[2]
    expert_result = jnp.einsum(
        "erf,efd->erd",
        lax.all_gather(hidden, "tp", axis=2, tiled=True),
        expert_down,
        preferred_element_type=jnp.float32,
    ).astype(jnp.bfloat16)
    returned = lax.all_to_all(expert_result, "ep", split_axis=1, concat_axis=0, tiled=True)
    flat_back = returned.reshape(expert_count * capacity, out_cols)
    picked = flat_back[slot_of].reshape(moe_tokens, TOPK, out_cols).astype(jnp.float32)
    mixing = group_weight[:, None] * expert_weight / jnp.sum(expert_weight, axis=1, keepdims=True)
    moe_out = jnp.sum(mixing[:, :, None] * picked, axis=1).astype(jnp.bfloat16)
    return (attended, moe_out)


def solution(mesh):
    placed = (
        P("ep", "tp"),
        P("ep", "tp"),
        P("ep", "tp"),
        P(),
        P(),
        P("ep", "tp"),
        P("ep", None),
        P("ep"),
        P("ep", None),
        P("ep", None, "tp"),
        P("ep", None, "tp"),
        P("ep", None, "tp"),
    )
    return jax.shard_map(
        on_device,
        mesh=mesh,
        in_specs=placed,
        out_specs=(P("ep", "tp"), P("ep", "tp")),
        check_vma=False,
    )
```

profile of v0, /device:TPU:0, one launch (start us, length us, event | category | flops | bytes accessed | tf_op | source)
XLA Modules:
  0.0 295.5 jit_solution(2823822702659321500)
XLA Ops:
  7.2 0.0 all-gather.7.cloned.1.call-start
  7.2 0.7 broadcast_multiply_fusion
  7.9 0.8 copy.47
  8.7 0.1 eq.31
  8.9 0.1 eq.27
  9.0 0.1 copy.46
  9.2 0.1 mul.255
  9.3 1.1 reduce-window.6
  10.5 0.2 slice_reduce_fusion
  10.7 0.1 fusion.36
  10.8 2.4 scatter_custom_fusion
  13.3 1.1 concatenate.11
  14.4 2.8 gather_fusion
  17.2 0.0 copy-start.3
  17.2 0.0 copy-start.7
  17.2 0.0 copy-start.4
  17.2 44.2 %all_to_all.21 = bf16[8,96,1024]{2,1,0:T(8,128)(2,1)} all-to-all(bf16[8,96,1024]{2,1,0:T(8,128)(2,1)S(1)} %bitcast.104), channel_id=1, replica_groups=mesh['ep'=8,'tp'=4] {'ep'}, dimensions={0} | all-to-all | bytes 3145728 | tf_op jit(solution)/shard_map/all_to_all | solution.py:118
  61.4 0.0 all-gather.7.cloned.1.call-update
  61.5 0.0 all-gather.5.cloned.1.call-start
  61.5 0.0 copy-done.3
  61.5 0.1 copy.42
  61.6 0.1 mul.220
  61.7 0.1 copy.41
  61.9 0.2 multiply_cosine_fusion
  62.1 0.1 multiply_multiply_fusion.1
  62.3 0.7 pad_maximum_fusion.1
  63.0 0.0 all-gather.5.cloned.1.call-update
  63.1 0.2 all-gather.9.cloned.1.call-start
  63.3 67.3 %all-gather.7.cloned.1.call-done = bf16[1,768,4096]{2,1,0:T(8,128)(2,1)} async-done(((bf16[1,768,1024]{2,1,0:T(8,128)(2,1)}), bf16[1,768,4096]{2,1,0:T(8,128)(2,1)}) %all-gather.7.cloned.1.call-update) | async-done | bytes 6291472 | tf_op jit(solution)/shard_map/all_gather | solution.py:125
  130.6 4.2 %multiply_reduce_fusion = f32[768]{0:T(1024)S(1)} fusion(bf16[1,768,4096]{2,1,0:T(8,128)(2,1)} %all-gather.7.cloned.1.call-done), kind=kLoop, calls=%fused_computation.9 | loop fusion | flops 9436416 | bytes 6294528 | tf_op jit(solution)/shard_map/reduce_sum | solution.py:129
  134.8 0.4 copy-done
  135.2 5.5 %fusion.5 = f32[768,512]{1,0:T(8,128)S(1)} fusion(bf16[1,768,4096]{2,1,0:T(8,128)(2,1)S(1)} %copy-done, bf16[1,4096,512]{2,1,0:T(8,128)(2,1)} %param.22), kind=kOutput, calls=%fused_computation.10 | convolution fusion | flops 3221225472 | bytes 12058624 | tf_op jit(solution)/shard_map/erd,edf->erf/dot_general | solution.py:128
  140.7 0.0 copy-done.9
  140.7 0.0 copy-start.8
  140.7 0.0 copy-start.2
  140.7 0.0 copy-start.5
  140.8 0.0 copy-start.6
  140.8 4.6 %multiply_convert_fusion = bf16[768,512]{1,0:T(8,128)(2,1)} fusion(f32[768,512]{1,0:T(8,128)S(1)} %fusion.5, bf16[1,4096,512]{2,1,0:T(8,128)(2,1)S(1)} %copy-done.9, bf16[1,768,4096]{2,1,0:T(8,128)(2,1)S(1)} %copy-done, f32[768]{0:T(1024)S(1)} %add_rsqrt_fusion.1), kind=kOutput, calls=%fused_computation.21 | convolution fusion | flops 3224371200 | bytes 12848128 | tf_op jit(solution)/shard_map/erd,edf->erf/dot_general | solution.py:127
  145.4 0.0 all-gather.9.cloned.1.call-update
  145.4 0.1 mul.237
  145.5 0.2 copy.43
  145.8 0.1 copy.45
  145.9 0.1 bitcast_reduce_fusion.1
  146.1 0.2 multiply_multiply_fusion
  146.3 0.2 subtract_convert_fusion
  146.5 16.9 %all-gather.5.cloned.1.call-done = bf16[2048,512]{0,1:T(8,128)(2,1)} async-done(((bf16[256,512]{0,1:T(8,128)(2,1)}), bf16[2048,512]{0,1:T(8,128)(2,1)}) %all-gather.5.cloned.1.call-update) | async-done | bytes 2097168 | tf_op jit(solution)/shard_map/all_gather | solution.py:93
  163.4 2.7 fusion.44
  166.1 14.0 %bitcast_reduce_fusion = (f32[4,4,256]{2,1,0:T(4,128)S(1)}, f32[4,2048,256,4]{2,1,3,0:T(8,128)}) fusion(bf16[2048,4,64,1]{0,2,3,1:T(8,128)(2,1)S(1)} %bitcast.107, bf16[256,4,4,64]{0,3,2,1:T(8,128)(2,1)S(1)} %bitcast.108), kind=kOutput, calls=%fused_computation.4 | convolution fusion | flops 1090514944 | bytes 35143680 | tf_op jit(solution)/shard_map/tkgd,skd->kgts/dot_general | solution.py:39
  180.1 27.9 %all-gather.9.cloned.1.call-done = bf16[768,2048]{1,0:T(8,128)(2,1)} async-done(((bf16[768,512]{1,0:T(8,128)(2,1)}), bf16[768,2048]{1,0:T(8,128)(2,1)}) %all-gather.9.cloned.1.call-update) | async-done | bytes 3145744 | tf_op jit(solution)/shard_map/all_gather | solution.py:135
  208.0 6.6 %fusion.16 = bf16[1,768,1024]{2,1,0:T(8,128)(2,1)S(1)} fusion(bf16[768,2048]{1,0:T(8,128)(2,1)} %all-gather.9.cloned.1.call-done, bf16[1,2048,1024]{2,1,0:T(8,128)(2,1)} %param.23), kind=kOutput, calls=%fused_computation.22 | convolution fusion | flops 3222011904 | bytes 8912896 | tf_op jit(solution)/shard_map/erf,efd->erd/dot_general | solution.py:133
  214.5 2.4 copy.58
  217.0 0.5 broadcast.321
  217.5 11.2 %reduce.3 = bf16[768,1024]{1,0:T(8,128)(2,1)} reduce(bf16[768,1,1024]{2,1,0:T(2,128)(2,1)S(1)} %bitcast.101, bf16[]{:T(256)} %broadcast.321), dimensions={1}, to_apply=%bitcast.99.reduce_sub_computation | reduce | bytes 3145730
  228.7 4.1 %reshape.311 = bf16[8,2,49152]{2,1,0:T(2,128)(2,1)} reshape(bf16[768,1024]{1,0:T(8,128)(2,1)} %reduce.3) | data formatting | bytes 3145728
  232.8 4.6 %all-to-all-start.1 = ((bf16[8,2,49152]{2,1,0:T(2,128)(2,1)}), bf16[8,2,49152]{2,1,0:T(2,128)(2,1)S(1)}, u32[]{:S(2)}, u32[]{:S(2)}) async-start(bf16[8,2,49152]{2,1,0:T(2,128)(2,1)} %reshape.311), calls=%async_computation.1 | async-start | bytes 3145728 | tf_op jit(solution)/shard_map/all_to_all | solution.py:139
  237.4 13.6 %fusion.1 = f32[4,4,256]{2,1,0:T(4,128)S(1)} fusion(f32[4,2048,256,4]{2,1,3,0:T(8,128)} %get-tuple-element.19, f32[4,4,256]{2,1,0:T(4,128)S(1)} %get-tuple-element.18), kind=kLoop, calls=%fused_computation.6 | loop fusion | flops 25161728 | bytes 33587200 | tf_op jit(solution)/shard_map/reduce_sum | solution.py:45
  251.1 13.6 %fusion.32 = bf16[256,4,4,64]{0,3,2,1:T(8,128)(2,1)S(1)} fusion(bf16[2048,4,64,1]{0,2,3,1:T(8,128)(2,1)S(1)} %bitcast.106, f32[4,2048,256,4]{2,1,3,0:T(8,128)} %get-tuple-element.19, f32[4,4,256]{2,1,0:T(4,128)S(1)} %get-tuple-element.18, f32[256,4,4]{0,2,1:T(4,128)S(1)} %bitcast_add_fusion, f32[256,4,4]{0,2,1:T(4,128)S(1)} %multiply_bitcast_fusion), kind=kOutput, calls=%fused_computation.26 | convolution fusion | flops 1099694080 | bytes 35176448 | tf_op jit(solution)/shard_map/kgts,skd->kgtd/dot_general | solution.py:46
  264.7 1.0 copy.50
  265.7 9.5 %all-to-all-done.1 = bf16[8,2,49152]{2,1,0:T(2,128)(2,1)S(1)} async-done(((bf16[8,2,49152]{2,1,0:T(2,128)(2,1)}), bf16[8,2,49152]{2,1,0:T(2,128)(2,1)S(1)}, u32[]{:S(2)}, u32[]{:S(2)}) %all-to-all-start.1) | async-done | bytes 1572896 | tf_op jit(solution)/shard_map/all_to_all | solution.py:139
  275.2 3.9 %reshape.312 = bf16[768,1,1024]{2,1,0:T(2,128)(2,1)} reshape(bf16[8,2,49152]{2,1,0:T(2,128)(2,1)S(1)} %all-to-all-done.1) | data formatting | bytes 3145728
  279.2 2.5 copy.57
  281.7 2.1 gather_fusion.1
  283.7 1.3 reshape.278
  285.1 3.5 %multiply_reduce_fusion.1 = bf16[256,1024]{1,0:T(8,128)(2,1)} fusion(f32[256,2,1024]{2,1,0:T(2,128)S(1)} %reshape.278, f32[256,2]{1,0:T(8,128)S(1)} %copy.45), kind=kLoop, calls=%fused_computation.18 | loop fusion | flops 786432 | bytes 2623488 | tf_op jit(solution)/shard_map/reduce_sum | solution.py:143
  (32 shorter events, 0.4 us)
Async XLA Ops:
  7.2 123.4 %all-gather.7.cloned.1.call-start = ((), (), s32[]{:S(2)}) async-start(), calls=%async_computation.3 | async-start | bytes 7864320 | tf_op jit(solution)/shard_map/all_gather | solution.py:125
  17.2 44.3 %copy-start.3 = (bf16[256,256]{1,0:T(8,128)(2,1)S(1)}, bf16[256,256]{1,0:T(8,128)(2,1)}, u32[]{:S(2)}) copy-start(bf16[256,256]{1,0:T(8,128)(2,1)} %param.14) | copy-start | bytes 393220
  17.2 44.4 %copy-start.7 = (f32[64]{0:T(128)S(1)}, f32[64]{0:T(128)}, u32[]{:S(2)}) copy-start(f32[64]{0:T(128)} %param.16) | copy-start | bytes 772
  17.2 44.5 %copy-start.4 = (bf16[256,256]{1,0:T(8,128)(2,1)S(1)}, bf16[256,256]{1,0:T(8,128)(2,1)}, u32[]{:S(2)}) copy-start(bf16[256,256]{1,0:T(8,128)(2,1)} %param.13) | copy-start | bytes 393220
  61.5 101.9 %all-gather.5.cloned.1.call-start = ((), (), s32[]{:S(2)}) async-start(), calls=%async_computation.2 | async-start | bytes 2359296 | tf_op jit(solution)/shard_map/all_gather | solution.py:93
  63.1 144.9 %all-gather.9.cloned.1.call-start = ((), (), s32[]{:S(2)}) async-start(), calls=%async_computation.4 | async-start | bytes 3932160 | tf_op jit(solution)/shard_map/all_gather | solution.py:135
  130.6 4.6 %copy-start = (bf16[1,768,4096]{2,1,0:T(8,128)(2,1)S(1)}, bf16[1,768,4096]{2,1,0:T(8,128)(2,1)}, u32[]{:S(2)}) copy-start(bf16[1,768,4096]{2,1,0:T(8,128)(2,1)} %all-gather.7.cloned.1.call-done) | copy-start | bytes 18874372
  135.2 5.5 %copy-start.9 = (bf16[1,4096,512]{2,1,0:T(8,128)(2,1)S(1)}, bf16[1,4096,512]{2,1,0:T(8,128)(2,1)}, u32[]{:S(2)}) copy-start(bf16[1,4096,512]{2,1,0:T(8,128)(2,1)} %param.21) | copy-start | bytes 12582916
  140.7 4.7 %copy-start.8 = (f32[64]{0:T(128)S(1)}, f32[64]{0:T(128)}, u32[]{:S(2)}) copy-start(f32[64]{0:T(128)} %param.15) | copy-start | bytes 772
  140.7 4.8 %copy-start.2 = (bf16[256,1024]{1,0:T(8,128)(2,1)S(1)}, bf16[256,1024]{1,0:T(8,128)(2,1)}, u32[]{:S(2)}) copy-start(bf16[256,1024]{1,0:T(8,128)(2,1)} %param.12) | copy-start | bytes 1572868
  140.7 5.0 %copy-start.5 = (f32[256,2]{0,1:T(2,128)S(1)}, f32[256,2]{0,1:T(2,128)}, u32[]{:S(2)}) copy-start(f32[256,2]{0,1:T(2,128)} %param.20) | copy-start | bytes 6148
  140.8 5.0 %copy-start.6 = (f32[256]{0:T(256)S(1)}, f32[256]{0:T(256)}, u32[]{:S(2)}) copy-start(f32[256]{0:T(256)} %param.19) | copy-start | bytes 3076
  232.8 42.4 %all-to-all-start.1 = ((bf16[8,2,49152]{2,1,0:T(2,128)(2,1)}), bf16[8,2,49152]{2,1,0:T(2,128)(2,1)S(1)}, u32[]{:S(2)}, u32[]{:S(2)}) async-start(bf16[8,2,49152]{2,1,0:T(2,128)(2,1)} %reshape.311), calls=%async_computation.1 | async-start | bytes 3145728 | tf_op jit(solution)/shard_map/all_to_all | solution.py:139
  237.4 13.7 %copy-start.1 = (bf16[2048,256]{0,1:T(8,128)(2,1)S(1)}, bf16[2048,256]{0,1:T(8,128)(2,1)}, u32[]{:S(2)}) copy-start(bf16[2048,256]{0,1:T(8,128)(2,1)} %get-tuple-element.11) | copy-start | bytes 3145732
Sparse Core Ops, SparseCore 0:
  61.6 68.9 all-gather.6
  132.7 30.5 all-gather.4
  165.2 42.7 all-gather.8
where the time goes:
time: 299 us; the launch traced here: 296 us
  waiting for transfers between devices  122 us (41%)
  blocking collectives  44.2 us (15%)
  matrix products  44.2 us (15%)
  other arithmetic  36.3 us (12%)
  local copies, waits for them, and re-layouts  29.7 us (10%)
  between operations  14.6 us (5%)
  starting transfers between devices  4.9 us (2%)
    all_gather x1, waiting for transfers between devices, on_device(): portion = lax.all_gather(arrived, 'tp', axis=2, tiled=True)  67.3 us
    all_to_all x1, blocking collectives, on_device(): lax.all_to_all(padded[owner_of].reshape(expert_count, capacity, moe_rows....  44.2 us
    all_gather x1, waiting for transfers between devices, on_device(): lax.all_gather(hidden, 'tp', axis=2, tiled=True)  27.9 us
    all_gather x1, waiting for transfers between devices, on_device(): lax.all_gather(joined, 'ep', axis=0, tiled=True)  16.9 us
    dot_general x1, matrix products, attend_block(): jnp.einsum('tkgd,skd->kgts', query_rot, keys_part, preferred_element_type...  14 us
    unnamed x29, local copies, waits for them, and re-layouts  13.7 us
    reduce_sum x1, other arithmetic, attend_block(): denominator = denominator * factor + jnp.sum(weights, axis=-1)  13.6 us
    dot_general x1, matrix products, attend_block(): jnp.einsum('kgts,skd->kgtd', weights.astype(jnp.bfloat16), values_part, p...  13.6 us
  transfers between devices with their start and end apart: 4, of which 4 were waited for; matrix products, arithmetic and copies ran while one was open for 21% of the time, Pallas kernels for 0%

commit v1 on v0

v1 whole, which is shorter than its diff:
```python
import jax
import jax.numpy as jnp
from jax import lax
from jax.sharding import PartitionSpec as P

D = 4096
HEAD_DIM = 64
GRID_W = 64
TOPK = 2
CHUNKS = 2


def rotary_tables(position):
    pair_count = HEAD_DIM // 4
    grid_pos = jnp.stack([position // GRID_W, position % GRID_W], axis=-1).astype(jnp.float32)
    frequency = 10000.0 ** (-jnp.arange(pair_count, dtype=jnp.float32) / pair_count)
    angles = grid_pos[:, :, None] * frequency
    return (jnp.cos(angles), jnp.sin(angles))


def normed_rotated(rows_in, gain, cosine, sine_of):
    row_count, head_count = (rows_in.shape[0], rows_in.shape[1])
    pair_count = HEAD_DIM // 4
    scaled = rows_in * lax.rsqrt(jnp.mean(rows_in * rows_in, axis=-1, keepdims=True) + 1e-06) * gain
    parted = scaled.reshape(row_count, head_count, 2, 2, pair_count)
    first_half, second = (parted[:, :, :, 0, :], parted[:, :, :, 1, :])
    cos_b, sin_b = (cosine[:, None], sine_of[:, None])
    turned = jnp.stack(
        [first_half * cos_b - second * sin_b, second * cos_b + first_half * sin_b], axis=3
    )
    return turned.reshape(row_count, head_count, HEAD_DIM).astype(jnp.bfloat16)


def attention(query_rot, portion, kv_width):
    key_count = portion.shape[0]
    head_count = kv_width // HEAD_DIM
    keys_part = portion[:, :kv_width].reshape(key_count, head_count, HEAD_DIM)
    values_part = portion[:, kv_width:].reshape(key_count, head_count, HEAD_DIM)
    scores = jnp.einsum(
        "tkgd,skd->kgts", query_rot, keys_part, preferred_element_type=jnp.float32
    ) * HEAD_DIM ** (-0.5)
    weights = jnp.exp(scores - jnp.max(scores, axis=-1, keepdims=True))
    denominator = jnp.sum(weights, axis=-1)
    summed = jnp.einsum(
        "kgts,skd->kgtd",
        weights.astype(jnp.bfloat16),
        values_part,
        preferred_element_type=jnp.float32,
    )
    return summed / denominator[..., None]


def on_device(
    queries,
    keys,
    values,
    query_gain,
    key_gain,
    moe_rows,
    route_ids,
    group_weight,
    expert_weight,
    expert_gate,
    expert_up,
    expert_down,
):
    ep = lax.axis_size("ep")
    tp = lax.axis_size("tp")
    me = lax.axis_index("ep")
    moe_tokens, chan = moe_rows.shape
    total = moe_tokens * ep
    capacity = 3 * moe_tokens * TOPK // (2 * ep) * ep
    everyone = lax.all_gather(moe_rows, "ep", axis=0, tiled=True)
    mixing = group_weight[:, None] * expert_weight / jnp.sum(expert_weight, axis=1, keepdims=True)
    table = lax.all_gather(
        jnp.concatenate([route_ids.astype(jnp.float32), mixing], axis=1).T, "ep", axis=1, tiled=True
    )
    mine = table[:TOPK] == me.astype(jnp.float32)
    chosen = jnp.any(mine, axis=0)
    mix_here = jnp.sum(jnp.where(mine, table[TOPK:], 0.0), axis=0)
    flags = chosen.reshape(ep, moe_tokens).astype(jnp.bfloat16)
    upper = jnp.triu(jnp.ones((moe_tokens, moe_tokens), jnp.bfloat16), 1)
    inner = jnp.dot(flags, upper, preferred_element_type=jnp.float32)
    counts = jnp.sum(flags.astype(jnp.float32), axis=1)
    earlier = jnp.sum(jnp.where(jnp.arange(ep)[None, :] < jnp.arange(ep)[:, None], counts[None, :], 0.0), axis=1)
    slot = (inner + earlier[:, None]).reshape(total).astype(jnp.int32)
    slot = jnp.where(chosen, slot, -1)

    tok_rows = queries.shape[0]
    q_heads = queries.shape[1] // HEAD_DIM
    k_heads = keys.shape[1] // HEAD_DIM
    group_size = q_heads // k_heads
    position = me * tok_rows + jnp.arange(tok_rows, dtype=jnp.int32)
    cosine, sine_of = rotary_tables(position)
    key_rot = normed_rotated(
        keys.astype(jnp.float32).reshape(tok_rows, k_heads, HEAD_DIM), key_gain, cosine, sine_of
    )
    kv_width = k_heads * HEAD_DIM
    joined = jnp.concatenate([key_rot.reshape(tok_rows, kv_width), values], axis=1)
    query_rot = normed_rotated(
        queries.astype(jnp.float32).reshape(tok_rows, q_heads, HEAD_DIM),
        query_gain,
        cosine,
        sine_of,
    )
    query_rot = query_rot.reshape(tok_rows, k_heads, group_size, HEAD_DIM)

    rows = capacity // CHUNKS
    gate_w = expert_gate[0].reshape(tp, chan, -1)
    up_w = expert_up[0].reshape(tp, chan, -1)
    down_w = expert_down[0].reshape(tp, -1, expert_down.shape[2])
    picks = []
    for c in range(CHUNKS):
        one_hot = (
            slot[None, :] == (c * rows + jnp.arange(rows, dtype=jnp.int32))[:, None]
        ).astype(jnp.bfloat16)
        picks.append(
            jnp.dot(one_hot, everyone, preferred_element_type=jnp.float32).astype(jnp.bfloat16)
        )
    gathered = [lax.all_gather(picks[0], "tp", axis=0)]
    kv_all = lax.all_gather(joined, "ep", axis=0, tiled=True)
    for c in range(1, CHUNKS):
        gathered.append(lax.all_gather(picks[c], "tp", axis=0))
    results = []
    for c in range(CHUNKS):
        portion = gathered[c]
        widened = portion.astype(jnp.float32)
        square_sum = jnp.sum(widened * widened, axis=(0, 2))
        inv_rms = lax.rsqrt(square_sum / D + 1e-06)[:, None]
        gate_act = jnp.einsum("ard,adf->rf", portion, gate_w, preferred_element_type=jnp.float32)
        up_act = jnp.einsum("ard,adf->rf", portion, up_w, preferred_element_type=jnp.float32)
        hidden = (jax.nn.silu(gate_act * inv_rms) * (up_act * inv_rms)).astype(jnp.bfloat16)
        hidden_all = lax.all_gather(hidden, "tp", axis=0)
        results.append(
            jnp.einsum(
                "arf,afd->rd", hidden_all, down_w, preferred_element_type=jnp.float32
            ).astype(jnp.bfloat16)
        )
    result = jnp.concatenate(results, axis=0)
    back = (slot[:, None] == jnp.arange(capacity, dtype=jnp.int32)[None, :]).astype(jnp.bfloat16)
    spread = (
        jnp.dot(back, result, preferred_element_type=jnp.float32) * mix_here[:, None]
    ).astype(jnp.bfloat16)
    moe_out = lax.psum_scatter(spread, "ep", scatter_dimension=0, tiled=True)

    attended = (
        attention(query_rot, kv_all, kv_width)
        .transpose(2, 0, 1, 3)
        .reshape(tok_rows, q_heads * HEAD_DIM)
        .astype(jnp.bfloat16)
    )
    return (attended, moe_out)


def solution(mesh):
    placed = (
        P("ep", "tp"),
        P("ep", "tp"),
        P("ep", "tp"),
        P(),
        P(),
        P("ep", "tp"),
        P("ep", None),
        P("ep"),
        P("ep", None),
        P("ep", None, "tp"),
        P("ep", None, "tp"),
        P("ep", None, "tp"),
    )
    return jax.shard_map(
        on_device,
        mesh=mesh,
        in_specs=placed,
        out_specs=(P("ep", "tp"), P("ep", "tp")),
        check_vma=False,
    )
```

time: 299 us -> 310 us (1.037); the launches traced: 296 us -> 310 us
  waiting for transfers between devices: 122 us -> 184 us
  blocking collectives: 44.2 us -> 15.9 us
  local copies, waits for them, and re-layouts: 29.7 us -> 4.67 us
  matrix products: 44.2 us -> 66.8 us
  other arithmetic: 36.3 us -> 23.1 us
  starting transfers between devices: 4.9 us -> 0.47 us
    all_gather x3 -> x6, waiting for transfers between devices: 112 us -> 176 us  [the longest x2 49.4 us: on_device(): hidden_all = lax.all_gather(hidden, 'tp', axis=0)]
    all_to_all x1 -> x0, blocking collectives: 44.2 us -> none  [on_device(): lax.all_to_all(padded[owner_of].reshape(expert_count, capacity, moe_rows....]
    dot_general x5 -> x12, matrix products: 44.2 us -> 66.8 us  [the longest x1 13.9 us: attention(): jnp.einsum('kgts,skd->kgtd', weights.astype(jnp.bfloat16), values_part, p...]
    all_gather x0 -> x1, blocking collectives: none -> 15.9 us  [on_device(): lax.all_gather(jnp.concatenate([route_ids.astype(jnp.float32), mixing], a...]
    unnamed x1 -> x0, other arithmetic: 11.2 us -> none
    unnamed x29 -> x23, local copies, waits for them, and re-layouts: 13.7 us -> 2.82 us
    all_to_all x1 -> x0, waiting for transfers between devices: 9.54 us -> none  [on_device(): lax.all_to_all(expert_result, 'ep', split_axis=1, concat_axis=0, tiled=True)]
    reduce_scatter x0 -> x1, waiting for transfers between devices: none -> 7.8 us  [on_device(): moe_out = lax.psum_scatter(spread, 'ep', scatter_dimension=0, tiled=True)]
  transfers between devices with their start and end apart: 4 -> 7, of which waited for: 4 -> 7; matrix products, arithmetic and copies ran while one was open for 21% -> 28% of each run, Pallas kernels for 0% -> 0%
where the time goes in v1:
time: 310 us
  waiting for transfers between devices  184 us (59%)
  matrix products  66.8 us (22%)
  other arithmetic  23.1 us (7%)
  blocking collectives  15.9 us (5%)
  between operations  14.4 us (5%)
  local copies, waits for them, and re-layouts  4.67 us (2%)
    all_gather x2, waiting for transfers between devices, on_device(): hidden_all = lax.all_gather(hidden, 'tp', axis=0)  49.4 us
    all_gather x1, waiting for transfers between devices, on_device(): gathered.append(lax.all_gather(picks[c], 'tp', axis=0))  37.8 us
    all_gather x1, waiting for transfers between devices, on_device(): gathered = [lax.all_gather(picks[0], 'tp', axis=0)]  35.2 us
    all_gather x1, waiting for transfers between devices, on_device(): everyone = lax.all_gather(moe_rows, 'ep', axis=0, tiled=True)  32.8 us
    all_gather x1, waiting for transfers between devices, on_device(): kv_all = lax.all_gather(joined, 'ep', axis=0, tiled=True)  20.7 us
    all_gather x1, blocking collectives, on_device(): lax.all_gather(jnp.concatenate([route_ids.astype(jnp.float32), mixing], a...  15.9 us
    dot_general x1, matrix products, attention(): jnp.einsum('kgts,skd->kgtd', weights.astype(jnp.bfloat16), values_part, p...  13.9 us
    reduce_sum x1, other arithmetic, attention(): denominator = jnp.sum(weights, axis=-1)  13.8 us
  transfers between devices with their start and end apart: 7, of which 7 were waited for; matrix products, arithmetic and copies ran while one was open for 28% of the time, Pallas kernels for 0%

profile of v1, /device:TPU:0, one launch (start us, length us, event | category | flops | bytes accessed | tf_op | source)
XLA Modules:
  0.0 309.8 jit_solution(2072310717542444445)
XLA Ops:
  7.2 0.0 all-gather.13.cloned.1.call-start
  7.2 0.7 all-gather.13.cloned.1.call-update
  7.9 0.0 all-gather.19.cloned.1.call-start
  7.9 0.7 convert_element_type.96
  8.6 0.7 reduce_sum.84
  9.3 0.7 multiply_divide_fusion
  10.0 15.9 %all_gather.34 = f32[4,2048]{1,0:T(4,128)S(1)} all-gather(f32[4,256]{1,0:T(4,128)S(1)} %maximum_bitcast_fusion), channel_id=1, replica_groups=mesh['ep'=8,'tp'=4] {'ep'}, dimensions={1}, use_global_device_ids=true | all-gather | bytes 36864 | tf_op jit(solution)/shard_map/all_gather | solution.py:75
  26.0 0.1 convert_reduce_fusion
  26.1 0.1 select_reduce_fusion
  26.2 0.1 fusion.38
  26.4 32.8 %all-gather.13.cloned.1.call-done = bf16[2048,1024]{1,0:T(8,128)(2,1)} async-done(((bf16[256,1024]{1,0:T(8,128)(2,1)}), bf16[2048,1024]{1,0:T(8,128)(2,1)}) %all-gather.13.cloned.1.call-update) | async-done | bytes 4194320 | tf_op jit(solution)/shard_map/all_gather | solution.py:73
  59.2 5.0 %fusion.16 = bf16[384,1024]{1,0:T(8,128)(2,1)} fusion(bf16[2048,1024]{1,0:T(8,128)(2,1)} %all-gather.13.cloned.1.call-done, s32[2048]{0:T(1024)S(1)} %broadcast_select_fusion, s32[384]{0:T(512)S(1)} %iota_add_fusion), kind=kOutput, calls=%fused_computation.24 | convolution fusion | flops 1611792384 | bytes 4990464 | tf_op jit(solution)/shard_map/dot_general | solution.py:118
  64.2 0.0 all-gather.19.cloned.1.call-update
  64.2 0.0 all-gather.15.cloned.1.call-start
  64.3 4.9 %fusion.19 = bf16[384,1024]{1,0:T(8,128)(2,1)} fusion(bf16[2048,1024]{1,0:T(8,128)(2,1)} %all-gather.13.cloned.1.call-done, s32[2048]{0:T(1024)S(1)} %broadcast_select_fusion), kind=kOutput, calls=%fused_computation.25 | convolution fusion | flops 1611792384 | bytes 4988928 | tf_op jit(solution)/shard_map/dot_general | solution.py:118
  69.1 0.0 all-gather.15.cloned.1.call-update
  69.2 0.0 all-gather.21.cloned.1.call-start
  69.2 37.8 %all-gather.19.cloned.1.call-done = bf16[1536,1024]{1,0:T(8,128)(2,1)} async-done(((bf16[384,1024]{1,0:T(8,128)(2,1)}), bf16[1536,1024]{1,0:T(8,128)(2,1)}) %all-gather.19.cloned.1.call-update) | async-done | bytes 3145744 | tf_op jit(solution)/shard_map/all_gather | solution.py:123
  107.0 2.6 multiply_reduce_fusion
  109.6 0.0 copy-start.7
  109.6 5.1 %fusion.24 = f32[384,512]{1,0:T(8,128)S(1)} fusion(bf16[4,384,1024]{2,1,0:T(8,128)(2,1)} %bitcast.109, bf16[4,1024,512]{2,1,0:T(8,128)(2,1)} %bitcast.117, f32[384]{0:T(512)S(1)} %add_rsqrt_fusion.2), kind=kOutput, calls=%fused_computation.30 | convolution fusion | flops 1610809344 | bytes 8128000 | tf_op jit(solution)/shard_map/ard,adf->rf/dot_general | solution.py:130
  114.7 0.0 copy-done.1
  114.7 0.2 copy-done.7
  114.9 2.6 fusion.29
  117.5 0.0 all-gather.21.cloned.1.call-update
  117.5 0.0 all-gather.17.cloned.1.call-start
  117.6 35.2 %all-gather.15.cloned.1.call-done = bf16[1536,1024]{1,0:T(8,128)(2,1)} async-done(((bf16[384,1024]{1,0:T(8,128)(2,1)}), bf16[1536,1024]{1,0:T(8,128)(2,1)}) %all-gather.15.cloned.1.call-update) | async-done | bytes 3145744 | tf_op jit(solution)/shard_map/all_gather | solution.py:120
  152.7 2.6 multiply_reduce_fusion.1
  155.3 0.0 copy-start.8
  155.4 5.1 %fusion.26 = f32[384,512]{1,0:T(8,128)S(1)} fusion(bf16[4,384,1024]{2,1,0:T(8,128)(2,1)} %bitcast.106, bf16[4,1024,512]{2,1,0:T(8,128)(2,1)} %bitcast.118, f32[384]{0:T(512)S(1)} %add_rsqrt_fusion.3), kind=kOutput, calls=%fused_computation.34 | convolution fusion | flops 1610809344 | bytes 8128000 | tf_op jit(solution)/shard_map/ard,adf->rf/dot_general | solution.py:130
  160.4 0.0 copy-done
  160.4 0.2 copy-done.8
  160.6 2.6 fusion.30
  163.2 0.0 all-gather.17.cloned.1.call-update
  163.3 0.0 all-gather.11.cloned.1.call-start
  163.3 0.1 copy.27
  163.4 0.0 copy-done.5
  163.4 0.1 mul.215
  163.5 0.1 copy.26
  163.7 0.2 multiply_cosine_fusion
  163.9 0.1 multiply_multiply_fusion.1
  164.1 0.8 pad_maximum_fusion.1
  164.9 0.0 all-gather.11.cloned.1.call-update
  164.9 0.2 reduce-scatter.2.cloned.1.call-start
  165.2 20.7 %all-gather.21.cloned.1.call-done = bf16[1536,512]{1,0:T(8,128)(2,1)} async-done(((bf16[384,512]{1,0:T(8,128)(2,1)}), bf16[1536,512]{1,0:T(8,128)(2,1)}) %all-gather.21.cloned.1.call-update) | async-done | bytes 1572880 | tf_op jit(solution)/shard_map/all_gather | solution.py:133
  185.9 4.5 %bitcast_convert_fusion = bf16[384,1024]{1,0:T(8,128)(2,1)S(1)} fusion(bf16[4,384,512]{2,1,0:T(8,128)(2,1)} %bitcast.123, bf16[4,512,1024]{2,1,0:T(8,128)(2,1)} %bitcast.121), kind=kOutput, calls=%fused_computation.19 | convolution fusion | flops 1611005952 | bytes 6553600 | tf_op jit(solution)/shard_map/arf,afd->rd/dot_general | solution.py:135
  190.3 28.7 %all-gather.17.cloned.1.call-done = bf16[1536,512]{1,0:T(8,128)(2,1)} async-done(((bf16[384,512]{1,0:T(8,128)(2,1)}), bf16[1536,512]{1,0:T(8,128)(2,1)}) %all-gather.17.cloned.1.call-update) | async-done | bytes 1572880 | tf_op jit(solution)/shard_map/all_gather | solution.py:133
  219.0 4.5 %bitcast_convert_fusion.1 = bf16[384,1024]{1,0:T(8,128)(2,1)S(1)} fusion(bf16[4,384,512]{2,1,0:T(8,128)(2,1)} %bitcast.124, bf16[4,512,1024]{2,1,0:T(8,128)(2,1)} %bitcast.122), kind=kOutput, calls=%fused_computation.20 | convolution fusion | flops 1611005952 | bytes 6553600 | tf_op jit(solution)/shard_map/arf,afd->rd/dot_general | solution.py:135
  223.5 5.1 %multiply_convert_fusion = bf16[2048,1024]{1,0:T(8,128)(2,1)} fusion(f32[2048]{0:T(1024)S(1)} %fusion.43, s32[2048]{0:T(1024)S(1)} %broadcast_select_fusion, bf16[384,1024]{1,0:T(8,128)(2,1)S(1)} %bitcast_convert_fusion, bf16[384,1024]{1,0:T(8,128)(2,1)S(1)} %bitcast_convert_fusion.1), kind=kOutput, calls=%fused_computation.6 | convolution fusion | flops 3230138368 | bytes 5783552 | tf_op jit(solution)/shard_map/dot_general | solution.py:142
  228.6 0.0 reduce-scatter.2.cloned.1.call-update
  228.6 0.6 copy-done.6
  229.2 0.1 mul.232
  229.3 0.3 copy-done.2
  229.6 0.2 copy.28
  229.8 0.1 bitcast_reduce_fusion.1
  230.0 0.2 multiply_multiply_fusion
  230.2 0.2 subtract_convert_fusion
  230.4 20.7 %all-gather.11.cloned.1.call-done = bf16[2048,512]{0,1:T(8,128)(2,1)} async-done(((bf16[256,512]{0,1:T(8,128)(2,1)}), bf16[2048,512]{0,1:T(8,128)(2,1)}) %all-gather.11.cloned.1.call-update) | async-done | bytes 2097168 | tf_op jit(solution)/shard_map/all_gather | solution.py:121
  251.1 1.7 fusion.49
  252.8 13.6 %bitcast_reduce_fusion = (f32[4,4,256]{2,1,0:T(4,128)S(1)}, f32[4,2048,256,4]{2,1,3,0:T(8,128)}) fusion(bf16[2048,4,64,1]{0,2,3,1:T(8,128)(2,1)S(1)} %bitcast.104, bf16[256,4,4,64]{0,3,2,1:T(8,128)(2,1)S(1)} %bitcast.111), kind=kOutput, calls=%fused_computation.1 | convolution fusion | flops 1090514944 | bytes 35143680 | tf_op jit(solution)/shard_map/tkgd,skd->kgts/dot_general | solution.py:39
  266.4 13.8 %fusion.1 = f32[4,4,256]{2,1,0:T(4,128)S(1)} fusion(f32[4,2048,256,4]{2,1,3,0:T(8,128)} %get-tuple-element.17, f32[4,4,256]{2,1,0:T(4,128)S(1)} %get-tuple-element.16), kind=kLoop, calls=%fused_computation.3 | loop fusion | flops 25161728 | bytes 33587200 | tf_op jit(solution)/shard_map/reduce_sum | solution.py:43
  280.2 13.9 %fusion.34 = bf16[256,4,4,64]{0,3,2,1:T(8,128)(2,1)S(1)} fusion(bf16[2048,4,64,1]{0,2,3,1:T(8,128)(2,1)S(1)} %bitcast.103, f32[4,2048,256,4]{2,1,3,0:T(8,128)} %get-tuple-element.17, f32[4,4,256]{2,1,0:T(4,128)S(1)} %get-tuple-element.16, f32[256,4,4]{0,2,1:T(4,128)S(1)} %bitcast.115), kind=kOutput, calls=%fused_computation.40 | convolution fusion | flops 1099431936 | bytes 35160064 | tf_op jit(solution)/shard_map/kgts,skd->kgtd/dot_general | solution.py:44
  294.1 1.0 copy.30
  295.1 7.8 %reduce-scatter.2.cloned.1.call-done = bf16[256,1024]{1,0:T(8,128)(2,1)} async-done(((bf16[2048,1024]{1,0:T(8,128)(2,1)}), bf16[256,1024]{1,0:T(8,128)(2,1)}) %reduce-scatter.2.cloned.1.call-update) | async-done | bytes 524304 | tf_op jit(solution)/shard_map/reduce_scatter | solution.py:144
  (27 shorter events, 0.4 us)
Async XLA Ops:
  7.2 52.1 %all-gather.13.cloned.1.call-start = ((), (), s32[]{:S(2)}) async-start(), calls=%async_computation.2 | async-start | bytes 4718592 | tf_op jit(solution)/shard_map/all_gather | solution.py:73
  7.9 99.1 %all-gather.19.cloned.1.call-start = ((), (), s32[]{:S(2)}) async-start(), calls=%async_computation.6 | async-start | bytes 3932160 | tf_op jit(solution)/shard_map/all_gather | solution.py:123
  64.2 88.5 %all-gather.15.cloned.1.call-start = ((), (), s32[]{:S(2)}) async-start(), calls=%async_computation.4 | async-start | bytes 3932160 | tf_op jit(solution)/shard_map/all_gather | solution.py:120
  69.2 116.7 %all-gather.21.cloned.1.call-start = ((), (), s32[]{:S(2)}) async-start(), calls=%async_computation.7 | async-start | bytes 1966080 | tf_op jit(solution)/shard_map/all_gather | solution.py:133
  109.6 5.1 %copy-start.1 = (bf16[1536,1024]{1,0:T(8,128)(2,1)S(1)}, bf16[1536,1024]{1,0:T(8,128)(2,1)}, u32[]{:S(2)}) copy-start(bf16[1536,1024]{1,0:T(8,128)(2,1)} %all-gather.19.cloned.1.call-done) | copy-start | bytes 9437188
  109.6 5.3 %copy-start.7 = (bf16[1,4096,512]{2,1,0:T(8,128)(2,1)S(1)}, bf16[1,4096,512]{2,1,0:T(8,128)(2,1)}, u32[]{:S(2)}) copy-start(bf16[1,4096,512]{2,1,0:T(8,128)(2,1)} %param.22) | copy-start | bytes 12582916
  117.5 101.5 %all-gather.17.cloned.1.call-start = ((), (), s32[]{:S(2)}) async-start(), calls=%async_computation.5 | async-start | bytes 1966080 | tf_op jit(solution)/shard_map/all_gather | solution.py:133
  155.3 5.1 %copy-start = (bf16[1536,1024]{1,0:T(8,128)(2,1)S(1)}, bf16[1536,1024]{1,0:T(8,128)(2,1)}, u32[]{:S(2)}) copy-start(bf16[1536,1024]{1,0:T(8,128)(2,1)} %all-gather.15.cloned.1.call-done) | copy-start | bytes 9437188
  155.3 5.3 %copy-start.8 = (bf16[1,4096,512]{2,1,0:T(8,128)(2,1)S(1)}, bf16[1,4096,512]{2,1,0:T(8,128)(2,1)}, u32[]{:S(2)}) copy-start(bf16[1,4096,512]{2,1,0:T(8,128)(2,1)} %param.22) | copy-start | bytes 12582916
  160.6 2.7 copy-start.3
  160.6 2.8 copy-start.5
  160.6 2.9 copy-start.4
  163.3 87.8 %all-gather.11.cloned.1.call-start = ((), (), s32[]{:S(2)}) async-start(), calls=%async_computation.1 | async-start | bytes 2359296 | tf_op jit(solution)/shard_map/all_gather | solution.py:121
  164.9 138.0 %reduce-scatter.2.cloned.1.call-start = ((), (), s32[]{:S(2)}) async-start(), calls=%async_computation.3 | async-start | bytes 4718592 | tf_op jit(solution)/shard_map/reduce_scatter | solution.py:144
  228.6 0.7 copy-start.6
  228.6 1.1 copy-start.2
Sparse Core Ops, SparseCore 0:
  9.6 49.6 all-gather.12
  64.4 42.6 all-gather.18
  108.9 43.8 all-gather.14
  155.0 30.8 all-gather.20
  188.1 30.8 all-gather.16
  220.5 30.5 all-gather.10
  254.0 48.9 reduce-scatter.1

commit v2 on v0

--- a/solution.py
+++ b/solution.py
@@ -1,6 +1,8 @@
 import jax
 import jax.numpy as jnp
 from jax import lax
+from jax.experimental import pallas as pl
+from jax.experimental.pallas import tpu as pltpu
 from jax.sharding import PartitionSpec as P
 
 D = 4096
@@ -52,7 +54,7 @@
     return (new_max, denominator, summed)
 
 
-def on_device(
+def plain_on_device(
     queries,
     keys,
     values,
@@ -144,6 +146,377 @@
     return (attended, moe_out)
 
 
+MESH = pl.DeviceIdType.MESH
+
+
+def flip(index, mask, width):
+    out = 0
+    bit = 1
+    while bit < width:
+        a, b = (index // bit) % 2, (mask // bit) % 2
+        out = out + bit * (a + b - 2 * a * b)
+        bit *= 2
+    return out
+
+
+def rope_kernel(q_ref, k_ref, v_ref, qg_ref, kg_ref, cos_ref, sin_ref, qo_ref, kv_ref):
+    rows = q_ref.shape[0]
+    lane = lax.broadcasted_iota(jnp.int32, (rows, 128), 1)
+    one = lax.broadcasted_iota(jnp.int32, (128, 128), 0) // HEAD_DIM
+    two = lax.broadcasted_iota(jnp.int32, (128, 128), 1) // HEAD_DIM
+    spread = jnp.where(one == two, 1.0 / HEAD_DIM, 0.0).astype(jnp.float32)
+    first = lane % 32 < 16
+    low = lane < HEAD_DIM
+    cosine, sine_of = cos_ref[...], sin_ref[...]
+
+    def turned(x, gain):
+        x = x.astype(jnp.float32)
+        mean = jnp.dot(
+            x * x, spread, preferred_element_type=jnp.float32, precision=lax.Precision.HIGHEST
+        )
+        y = x * lax.rsqrt(mean + 1e-06) * gain
+        partner = jnp.where(first, pltpu.roll(y, 112, 1), pltpu.roll(y, 16, 1))
+        return y * cosine + partner * sine_of
+
+    q_slabs = q_ref.shape[1] // 128
+    k_slabs = k_ref.shape[1] // 128
+    per_kv = q_slabs // (2 * k_slabs)
+    for s in range(q_slabs):
+        r = turned(q_ref[:, s * 128 : (s + 1) * 128], qg_ref[...])
+        r = r.astype(jnp.bfloat16).astype(jnp.float32) * HEAD_DIM ** (-0.5)
+        moved = pltpu.roll(r, HEAD_DIM, 1)
+        if (s // per_kv) % 2 == 0:
+            pair = (jnp.where(low, r, 0.0), jnp.where(low, moved, 0.0))
+        else:
+            pair = (jnp.where(low, 0.0, moved), jnp.where(low, 0.0, r))
+        qo_ref[2 * s] = pair[0].astype(jnp.bfloat16)
+        qo_ref[2 * s + 1] = pair[1].astype(jnp.bfloat16)
+    for s in range(k_slabs):
+        kv_ref[s] = turned(k_ref[:, s * 128 : (s + 1) * 128], kg_ref[...]).astype(jnp.bfloat16)
+        kv_ref[k_slabs + s] = v_ref[:, s * 128 : (s + 1) * 128]
+
+
+def main_kernel(
+    ep, picks, kv, q_ref, s0_ref, s1_ref, mix_ref, wg_hbm, wu_hbm, wd_hbm,
+    att_ref, moe_ref,
+    xg, hid, res, ret, kvall, wg, wu, wd,
+    w_sem, d_send, d_recv, x_send, x_recv, xr_send, xr_recv,
+    h_send, h_recv, hr_send, hr_recv, r_send, r_recv, k_send, k_recv,
+):
+    me, tme = lax.axis_index("ep"), lax.axis_index("tp")
+    tx, ty = flip(tme, 1, 4), flip(tme, 2, 4)
+    sides = (tx, ty)
+    cap = picks.shape[1]
+    half = cap // 2
+    pairs = ep // 2
+    width = wg.shape[1]
+    chan = picks.shape[2]
+
+    weights = [
+        pltpu.make_async_copy(a, b, w_sem.at[n])
+        for n, (a, b) in enumerate(((wg_hbm.at[0], wg), (wu_hbm.at[0], wu), (wd_hbm.at[0], wd)))
+    ]
+    for copy in weights:
+        copy.start()
+    barrier = pltpu.get_barrier_semaphore()
+    for j in range(1, ep):
+        pl.semaphore_signal(barrier, inc=1, device_id={"ep": flip(me, j, ep)}, device_id_type=MESH)
+    for side in sides:
+        pl.semaphore_signal(barrier, inc=1, device_id={"tp": side}, device_id_type=MESH)
+    pl.semaphore_wait(barrier, ep + 1)
+
+    def remote(src, dst, send, recv, device):
+        return pltpu.make_async_remote_copy(
+            src_ref=src, dst_ref=dst, send_sem=send, recv_sem=recv,
+            device_id=device, device_id_type=MESH,
+        )
+
+    def dispatch(j):
+        to = flip(me, j, ep)
+        return remote(picks.at[to], xg.at[j, tme], d_send.at[j], d_recv.at[j], {"ep": to})
+
+    def keys_out(j):
+        return remote(kv, kvall.at[me], k_send.at[j], k_recv.at[j], {"ep": flip(me, j, ep)})
+
+    def keys_on(j):
+        block = flip(me, j - 1, ep)
+        return remote(
+            kvall.at[block], kvall.at[block], k_send.at[j], k_recv.at[j], {"ep": flip(me, 1, ep)}
+        )
+
+    def cross(c, n, src=None):
+        src = xg.at[c, tme] if src is None else src
+        return remote(src, xg.at[c, tme], x_send.at[c, n], x_recv.at[c, n], {"tp": sides[n]})
+
+    def cross_on(c, n):
+        part = xg.at[c, sides[n], pl.ds(n * half, half)]
+        return remote(part, part, xr_send.at[c, n], xr_recv.at[c, n], {"tp": sides[1 - n]})
+
+    def wide(i, n):
+        return remote(
+            hid.at[i, tme], hid.at[i, tme], h_send.at[i, n], h_recv.at[i, n], {"tp": sides[n]}
+        )
+
+    def wide_on(i, n):
+        part = hid.at[i, sides[n], pl.ds(n * cap, cap)]
+        return remote(part, part, hr_send.at[i, n], hr_recv.at[i, n], {"tp": sides[1 - n]})
+
+    def back(i, n):
+        c = 2 * i + n
+        return remote(
+            res.at[i, pl.ds(n * cap, cap)], ret.at[me], r_send.at[c], r_recv.at[c],
+            {"ep": flip(me, c, ep)},
+        )
+
+    for j in range(1, 4):
+        dispatch(j).start()
+    for j in range(1, ep):
+        if j == 1 or j % 2 == 0:
+            keys_out(j).start()
+    for j in range(4, ep):
+        dispatch(j).start()
+
+    xg[0, tme] = picks[me]
+    kvall[me] = kv[...]
+    for n in range(2):
+        cross(0, n, picks.at[me]).start()
+
+    def enter(c):
+        dispatch(c).wait_recv()
+        for n in range(2):
+            cross(c, n).start()
+
+    def relay(i):
+        for d in range(2):
+            for n in range(2):
+                cross(2 * i + d, n).wait_recv()
+                cross_on(2 * i + d, n).start()
+
+    for c in range(1, 4):
+        enter(c)
+    relay(0)
+    for copy in weights:
+        copy.wait()
+
+    def first_half(i):
+        for d in range(2):
+            for n in range(2):
+                cross_on(2 * i + d, n).wait_recv()
+        gate = jnp.zeros((2 * cap, width), jnp.float32)
+        up = jnp.zeros((2 * cap, width), jnp.float32)
+        square = jnp.zeros((2 * cap, 1), jnp.float32)
+        for a in range(4):
+            x = xg[pl.ds(2 * i, 2), a].reshape(2 * cap, chan)
+            w = x.astype(jnp.float32)
+            square = square + jnp.sum(w * w, axis=1, keepdims=True)
+            gate = gate + jnp.dot(
+                x, wg[a * chan : (a + 1) * chan, :], preferred_element_type=jnp.float32
+            )
+            up = up + jnp.dot(
+                x, wu[a * chan : (a + 1) * chan, :], preferred_element_type=jnp.float32
+            )
+        inv = lax.rsqrt(square / D + 1e-06)
+        g = gate * inv
+        hid[i, tme] = (g / (1.0 + jnp.exp(-g)) * (up * inv)).astype(jnp.bfloat16)
+        for n in range(2):
+            wide(i, n).start()
+
+    def second_half(i):
+        for n in range(2):
+            wide_on(i, n).wait_recv()
+        total = jnp.zeros((2 * cap, chan), jnp.float32)
+        for a in range(4):
+            total = total + jnp.dot(
+                hid[i, a], wd[a * width : (a + 1) * width, :], preferred_element_type=jnp.float32
+            )
+        res[i] = total.astype(jnp.bfloat16)
+
+        @pl.when(i > 0)
+        def _():
+            back(i, 0).start()
+
+        @pl.when(i == 0)
+        def _():
+            ret[me] = res[0, :cap]
+
+        back(i, 1).start()
+
+    heads = q_ref.shape[0]
+    slabs = heads // 2
+    k_slabs = kv.shape[0] // 2
+    per_kv = slabs // (2 * k_slabs)
+    keys_total = ep * kv.shape[1]
+
+    def attend(m, carry):
+        pp = m // (2 * per_kv)
+        k = kvall[:, pp].reshape(keys_total, 128)
+        v = kvall[:, k_slabs + pp].reshape(keys_total, 128)
+        outs = []
+        for d in range(2):
+            s = lax.dot_general(
+                q_ref[2 * m + d], k, (((1,), (1,)), ((), ())), preferred_element_type=jnp.float32
+            )
+            p = jnp.exp(s - jnp.max(s, axis=1, keepdims=True))
+            den = jnp.sum(p, axis=1, keepdims=True)
+            o = jnp.dot(p.astype(jnp.bfloat16), v, preferred_element_type=jnp.float32)
+            outs.append(o / den)
+        low = lax.broadcasted_iota(jnp.int32, outs[0].shape, 1) < HEAD_DIM
+        even = jnp.where(low, outs[0], pltpu.roll(outs[1], HEAD_DIM, 1))
+        odd = jnp.where(low, pltpu.roll(outs[0], HEAD_DIM, 1), outs[1])
+        side = ((m // per_kv) % 2).astype(jnp.float32)
+        both = jnp.where(side == 0.0, even, odd)
+        att_ref[:, pl.ds(pl.multiple_of(m * 128, 128), 128)] = both.astype(jnp.bfloat16)
+        return carry
+
+    def keys_relay():
+        for j in range(2, ep, 2):
+            keys_out(j).wait_recv()
+            keys_on(j + 1).start()
+
+    def keys_ready():
+        keys_out(1).wait_recv()
+        for j in range(2, ep, 2):
+            keys_on(j + 1).wait_recv()
+
+    def step(i, carry):
+        first_half(i)
+
+        @pl.when(i < pairs - 1)
+        def _():
+            relay(i + 1)
+
+        @pl.when(i == 0)
+        def _():
+            keys_relay()
+
+        @pl.when(i == 1)
+        def _():
+            keys_ready()
+
+        @pl.when(i < pairs - 2)
+        def _():
+            enter(2 * i + 4)
+            enter(2 * i + 5)
+
+        begin = slabs * jnp.maximum(i - 1, 0) * 2 // 5
+        begin = jnp.where(i == pairs - 1, slabs - 1, begin)
+        end = jnp.where(i == 0, 0, slabs * i * 2 // 5)
+        end = jnp.where(i == pairs - 2, slabs - 1, end)
+        end = jnp.where(i == pairs - 1, slabs, end)
+        lax.fori_loop(begin, end, attend, 0)
+        for n in range(2):
+            wide(i, n).wait_recv()
+            wide_on(i, n).start()
+        second_half(i)
+        return carry
+
+    lax.fori_loop(0, pairs, step, 0)
+
+    for c in range(1, ep):
+        back(c // 2, c % 2).wait_recv()
+    everything = ret[...].reshape(ep * cap, chan)
+    mix = mix_ref[...]
+    one = jnp.dot(s0_ref[...], everything, preferred_element_type=jnp.float32)
+    two = jnp.dot(s1_ref[...], everything, preferred_element_type=jnp.float32)
+    moe_ref[...] = (mix[:, 0:1] * one + mix[:, 1:2] * two).astype(jnp.bfloat16)
+
+    for c in range(ep):
+        for n in range(2):
+            cross(c, n).wait_send()
+            cross_on(c, n).wait_send()
+        if c > 0:
+            dispatch(c).wait_send()
+            back(c // 2, c % 2).wait_send()
+            keys_out(c).wait_send()
+    for i in range(pairs):
+        for n in range(2):
+            wide(i, n).wait_send()
+            wide_on(i, n).wait_send()
+
+
+def on_device(
+    queries, keys, values, query_gain, key_gain, moe_rows, route_ids, group_weight,
+    expert_weight, expert_gate, expert_up, expert_down,
+):
+    ep, tp = lax.axis_size("ep"), lax.axis_size("tp")
+    moe_tokens, chan = moe_rows.shape
+    cap = 3 * moe_tokens * TOPK // (2 * expert_gate.shape[0] * ep)
+    fits = tp == 4 and ep == 8 and cap % 32 == 0 and expert_gate.shape[0] == 1
+    if not fits or queries.shape[1] // 128 != 8 or keys.shape[1] // 128 != 2:
+        return plain_on_device(
+            queries, keys, values, query_gain, key_gain, moe_rows, route_ids, group_weight,
+            expert_weight, expert_gate, expert_up, expert_down,
+        )
+    tok = queries.shape[0]
+    position = lax.axis_index("ep") * tok + jnp.arange(tok, dtype=jnp.int32)
+    lane = jnp.arange(128, dtype=jnp.int32)
+    pair_count = HEAD_DIM // 4
+    frequency = 10000.0 ** (-(lane % pair_count).astype(jnp.float32) / pair_count)
+    on_rows = (lane // (2 * pair_count)) % 2 == 0
+    grid_pos = jnp.where(
+        on_rows[None, :], (position // GRID_W)[:, None], (position % GRID_W)[:, None]
+    ).astype(jnp.float32)
+    angles = grid_pos * frequency[None, :]
+    sign = jnp.where((lane // pair_count) % 2 == 0, -1.0, 1.0).astype(jnp.float32)
+    heads = queries.shape[1] // HEAD_DIM
+    slabs = keys.shape[1] // 128
+    q_turned, kv = pl.pallas_call(
+        rope_kernel,
+        out_shape=(
+            jax.ShapeDtypeStruct((heads, tok, 128), jnp.bfloat16),
+            jax.ShapeDtypeStruct((2 * slabs, tok, 128), jnp.bfloat16),
+        ),
+    )(
+        queries, keys, values,
+        jnp.tile(query_gain, 2)[None, :], jnp.tile(key_gain, 2)[None, :],
+        jnp.cos(angles), jnp.sin(angles) * sign[None, :],
+    )
+    picks_all = moe_tokens * TOPK
+    route_list = route_ids.reshape(picks_all)
+    one_hot = (route_list[:, None] == jnp.arange(ep, dtype=jnp.int32)[None, :]).astype(jnp.int32)
+    rank_of = jnp.sum((jnp.cumsum(one_hot, axis=0) - one_hot) * one_hot, axis=1)
+    slot_of = (route_list * cap + rank_of).reshape(moe_tokens, TOPK)
+    columns = jnp.arange(ep * cap, dtype=jnp.int32)[None, :]
+    picked = [(slot_of[:, n : n + 1] == columns).astype(jnp.bfloat16) for n in range(TOPK)]
+    sent = lax.dot_general(
+        picked[0] + picked[1], moe_rows, (((0,), (0,)), ((), ())),
+        preferred_element_type=jnp.float32,
+    ).astype(jnp.bfloat16).reshape(ep, cap, chan)
+    mixing = group_weight[:, None] * expert_weight / jnp.sum(expert_weight, axis=1, keepdims=True)
+    width = expert_gate.shape[2]
+    vmem = pl.BlockSpec(memory_space=pltpu.VMEM)
+    hbm = pl.BlockSpec(memory_space=pl.ANY)
+    dma = pltpu.SemaphoreType.DMA
+    bf = jnp.bfloat16
+    attended, moe_out = pl.pallas_call(
+        lambda *refs: main_kernel(ep, *refs),
+        out_shape=(
+            jax.ShapeDtypeStruct(queries.shape, bf),
+            jax.ShapeDtypeStruct(moe_rows.shape, bf),
+        ),
+        in_specs=[vmem] * 6 + [hbm] * 3,
+        out_specs=(vmem, vmem),
+        scratch_shapes=[
+            pltpu.VMEM((ep, tp, cap, chan), bf),
+            pltpu.VMEM((ep // 2, tp, 2 * cap, width), bf),
+            pltpu.VMEM((ep // 2, 2 * cap, chan), bf),
+            pltpu.VMEM((ep, cap, chan), bf),
+            pltpu.VMEM((ep, 2 * slabs, tok, 128), bf),
+            pltpu.VMEM(expert_gate.shape[1:], bf),
+            pltpu.VMEM(expert_up.shape[1:], bf),
+            pltpu.VMEM(expert_down.shape[1:], bf),
+            dma((3,)), dma((ep,)), dma((ep,)),
+            dma((ep, 2)), dma((ep, 2)), dma((ep, 2)), dma((ep, 2)),
+            dma((ep // 2, 2)), dma((ep // 2, 2)), dma((ep // 2, 2)), dma((ep // 2, 2)),
+            dma((ep,)), dma((ep,)), dma((ep,)), dma((ep,)),
+        ],
+        compiler_params=pltpu.CompilerParams(
+            collective_id=0, has_side_effects=True, vmem_limit_bytes=60 * 1024 * 1024
+        ),
+    )(sent, kv, q_turned, picked[0], picked[1], mixing, expert_gate, expert_up, expert_down)
+    return (attended, moe_out)
+
+
 def solution(mesh):
     placed = (
         P("ep", "tp"),

time: 299 us -> 151 us (0.51)
  the two profiles are of different devices: /device:TPU:0 before, /device:TPU:9 now
where the time goes in v2:
time: 151 us
  Pallas kernels  134 us (89%)
  local copies, waits for them, and re-layouts  8.02 us (5%)
  other arithmetic  5.79 us (4%)
  matrix products  1.92 us (1%)
    pallas_call x1, Pallas kernels, on_device(): pl.pallas_call(lambda *refs: main_kernel(ep, *refs), out_shape=(jax.Shape...  130 us
    unnamed x5, local copies, waits for them, and re-layouts  4.55 us
    pallas_call x1, Pallas kernels, on_device(): pl.pallas_call(rope_kernel, out_shape=(jax.ShapeDtypeStruct((heads, tok,...  3.67 us

profile of v2, /device:TPU:9, one launch (start us, length us, event | category | flops | bytes accessed | tf_op | source)
XLA Modules:
  0.0 150.5 jit_solution(5634990679905592297)
XLA Ops:
  0.6 0.0 copy-start
  0.7 0.7 tile.4
  1.4 0.7 broadcast_in_dim_tile.6.qg_ref
  2.0 0.7 tile.5
  2.7 0.6 broadcast_in_dim_tile.7.kg_ref
  3.3 0.7 fusion.17
  4.0 0.8 copy.28
  4.8 0.1 eq.79
  5.0 0.1 eq.75
  5.1 1.1 reduce-window.6
  6.3 0.2 slice_reduce_fusion
  6.5 0.1 fusion.7
  6.6 0.1 reduce_sum.21
  6.8 0.1 copy.30
  6.9 0.7 multiply_add_fusion
  7.6 0.1 copy.31
  7.7 0.8 broadcast_divide_fusion.refs_5_
  8.5 1.2 sine_multiply_fusion
  9.7 1.1 fusion
  10.8 3.7 %shard_map.131 = (bf16[16,256,128]{2,1,0:T(8,128)(2,1)}, bf16[4,256,128]{2,1,0:T(8,128)(2,1)}) custom-call(bf16[256,1024]{1,0:T(8,128)(2,1)} %q_ref.1, bf16[256,256]{1,0:T(8,128)(2,1)} %k_ref.1, bf16[256,256]{1,0:T(8,128)(2,1)} %v_ref.1, f32[1,128]{1,0:T(1,128)} %broadcast_in_dim_tile.6.qg_ref, f32[1,128]{1,0:T(1,128)} %broadcast_in_dim_tile.7.kg_ref, ...), custom_call_target="tpu_custom_call" | custom-call | tf_op jit(solution)/shard_map/pallas_call | solution.py:463
  14.4 0.0 copy-done
  14.4 1.9 %convolution_convert_fusion = bf16[768,1024]{1,0:T(8,128)(2,1)} fusion(bf16[256,1024]{1,0:T(8,128)(2,1)S(1)} %copy-done, s32[256]{0:T(256)S(1)} %bitcast.16, s32[256]{0:T(256)S(1)} %bitcast.14), kind=kOutput, calls=%fused_computation | convolution fusion | flops 405012480 | bytes 2099200 | tf_op jit(solution)/shard_map/dot_general | solution.py:481
  16.4 130.4 %shard_map.132 = (bf16[256,1024]{1,0:T(8,128)(2,1)}, bf16[256,1024]{1,0:T(8,128)(2,1)}) custom-call(bf16[8,96,1024]{2,1,0:T(8,128)(2,1)} %bitcast.12, bf16[4,256,128]{2,1,0:T(8,128)(2,1)} %get-tuple-element.4.refs_1_, bf16[16,256,128]{2,1,0:T(8,128)(2,1)} %get-tuple-element.5.refs_2_, bf16[256,768]{1,0:T(8,128)(2,1)} %get-tuple-element.16.refs_3_, ...), custom_call_target="tpu_custom_call" | custom-call | tf_op jit(solution)/shard_map/pallas_call | solution.py:491
  146.8 1.9 %copy.35 = bf16[256,1024]{1,0:T(8,128)(2,1)} copy(bf16[256,1024]{1,0:T(8,128)(2,1)} %get-tuple-element.20) | data formatting | bytes 1048576
  148.6 1.9 %copy.36 = bf16[256,1024]{1,0:T(8,128)(2,1)} copy(bf16[256,1024]{1,0:T(8,128)(2,1)} %get-tuple-element.21) | data formatting | bytes 1048576
  (7 shorter events, 0.1 us)
Async XLA Ops:
  0.6 13.8 %copy-start = (bf16[256,1024]{1,0:T(8,128)(2,1)S(1)}, bf16[256,1024]{1,0:T(8,128)(2,1)}, u32[]{:S(2)}) copy-start(bf16[256,1024]{1,0:T(8,128)(2,1)} %param.17) | copy-start | bytes 1572868

commit v3 on v2

--- a/solution.py
+++ b/solution.py
@@ -403,10 +403,19 @@
         end = jnp.where(i == 0, 0, slabs * i * 2 // 5)
         end = jnp.where(i == pairs - 2, slabs - 1, end)
         end = jnp.where(i == pairs - 1, slabs, end)
-        lax.fori_loop(begin, end, attend, 0)
-        for n in range(2):
-            wide(i, n).wait_recv()
-            wide_on(i, n).start()
+
+        def hidden_on():
+            for n in range(2):
+                wide(i, n).wait_recv()
+                wide_on(i, n).start()
+
+        def unit(m, carried):
+            attend(m, carried)
+            pl.when(m == begin)(hidden_on)
+            return carried
+
+        lax.fori_loop(begin, end, unit, 0)
+        pl.when(begin == end)(hidden_on)
         second_half(i)
         return carry
 

time: 151 us -> 150 us (level)
  the two profiles are of different devices: /device:TPU:9 before, /device:TPU:0 now
where the time goes in v3:
time: 150 us; the launch traced here: 148 us
  Pallas kernels  131 us (87%)
  local copies, waits for them, and re-layouts  8.02 us (5%)
  other arithmetic  5.79 us (4%)
  matrix products  1.92 us (1%)
    pallas_call x1, Pallas kernels, on_device(): pl.pallas_call(lambda *refs: main_kernel(ep, *refs), out_shape=(jax.Shape...  128 us
    unnamed x5, local copies, waits for them, and re-layouts  4.55 us
    pallas_call x1, Pallas kernels, on_device(): pl.pallas_call(rope_kernel, out_shape=(jax.ShapeDtypeStruct((heads, tok,...  3.67 us

profile of v3, /device:TPU:0, one launch (start us, length us, event | category | flops | bytes accessed | tf_op | source)
XLA Modules:
  0.0 147.7 jit_solution(9070953160071856340)
XLA Ops:
  0.6 0.0 copy-start
  0.7 0.7 tile.4
  1.4 0.7 broadcast_in_dim_tile.6.qg_ref
  2.0 0.7 tile.5
  2.7 0.6 broadcast_in_dim_tile.7.kg_ref
  3.3 0.7 fusion.17
  4.0 0.8 copy.28
  4.8 0.1 eq.79
  5.0 0.1 eq.75
  5.1 1.1 reduce-window.6
  6.3 0.2 slice_reduce_fusion
  6.5 0.1 fusion.7
  6.6 0.1 reduce_sum.21
  6.8 0.1 copy.30
  6.9 0.7 multiply_add_fusion
  7.6 0.1 copy.31
  7.7 0.8 broadcast_divide_fusion.refs_5_
  8.5 1.2 sine_multiply_fusion
  9.7 1.1 fusion
  10.8 3.7 %shard_map.131 = (bf16[16,256,128]{2,1,0:T(8,128)(2,1)}, bf16[4,256,128]{2,1,0:T(8,128)(2,1)}) custom-call(bf16[256,1024]{1,0:T(8,128)(2,1)} %q_ref.1, bf16[256,256]{1,0:T(8,128)(2,1)} %k_ref.1, bf16[256,256]{1,0:T(8,128)(2,1)} %v_ref.1, f32[1,128]{1,0:T(1,128)} %broadcast_in_dim_tile.6.qg_ref, f32[1,128]{1,0:T(1,128)} %broadcast_in_dim_tile.7.kg_ref, ...), custom_call_target="tpu_custom_call" | custom-call | tf_op jit(solution)/shard_map/pallas_call | solution.py:472
  14.4 0.0 copy-done
  14.4 1.9 %convolution_convert_fusion = bf16[768,1024]{1,0:T(8,128)(2,1)} fusion(bf16[256,1024]{1,0:T(8,128)(2,1)S(1)} %copy-done, s32[256]{0:T(256)S(1)} %bitcast.16, s32[256]{0:T(256)S(1)} %bitcast.14), kind=kOutput, calls=%fused_computation | convolution fusion | flops 405012480 | bytes 2099200 | tf_op jit(solution)/shard_map/dot_general | solution.py:490
  16.4 127.6 %shard_map.132 = (bf16[256,1024]{1,0:T(8,128)(2,1)}, bf16[256,1024]{1,0:T(8,128)(2,1)}) custom-call(bf16[8,96,1024]{2,1,0:T(8,128)(2,1)} %bitcast.12, bf16[4,256,128]{2,1,0:T(8,128)(2,1)} %get-tuple-element.4.refs_1_, bf16[16,256,128]{2,1,0:T(8,128)(2,1)} %get-tuple-element.5.refs_2_, bf16[256,768]{1,0:T(8,128)(2,1)} %get-tuple-element.16.refs_3_, ...), custom_call_target="tpu_custom_call" | custom-call | tf_op jit(solution)/shard_map/pallas_call | solution.py:500
  143.9 1.9 %copy.35 = bf16[256,1024]{1,0:T(8,128)(2,1)} copy(bf16[256,1024]{1,0:T(8,128)(2,1)} %get-tuple-element.20) | data formatting | bytes 1048576
  145.8 1.9 %copy.36 = bf16[256,1024]{1,0:T(8,128)(2,1)} copy(bf16[256,1024]{1,0:T(8,128)(2,1)} %get-tuple-element.21) | data formatting | bytes 1048576
  (7 shorter events, 0.1 us)
Async XLA Ops:
  0.6 13.8 %copy-start = (bf16[256,1024]{1,0:T(8,128)(2,1)S(1)}, bf16[256,1024]{1,0:T(8,128)(2,1)}, u32[]{:S(2)}) copy-start(bf16[256,1024]{1,0:T(8,128)(2,1)} %param.17) | copy-start | bytes 1572868
